TPU v7x, 32 devices: a whole 2x2x4 slice. The times are simulated.
32 devices in a mesh: ep: 8 (over z, core), tp: 4 (over y, x).
Axes of the slice: x: 2, y: 2, z: 4, core: 2. Of those that a mesh axis runs over, the one named last changes fastest.
Arguments:
- tokens: bfloat16 [64, 2048], P('ep'), may hold values from -6 to 6
- attn_gain: float32 [2048], replicated, may hold values from 0.1 to 1.9
- query_weight: bfloat16 [2048, 4096], P('ep', 'tp'), may hold values from -0.125 to 0.125
- key_weight: bfloat16 [2048, 4096], P('ep', 'tp'), may hold values from -0.125 to 0.125
- value_weight: bfloat16 [2048, 4096], P('ep', 'tp'), may hold values from -0.125 to 0.125
- query_gain: float32 [128], replicated, may hold values from 0.1 to 1.9
- stick_bias: float32 [32], P('tp'), may hold values from -7 to -2.5
- key_cache: bfloat16 [64, 32, 512, 128], P('ep', 'tp'), may hold values from -6 to 6
- value_cache: bfloat16 [64, 32, 512, 128], P('ep', 'tp'), may hold values from -6 to 6
- lengths: int32 [64], P('ep'), may hold values from 64 to 512, as said below
- out_weight: bfloat16 [4096, 2048], P('tp'), may hold values from -0.375 to 0.375
- mix_gain: float32 [2048], replicated, may hold values from 0.1 to 1.9
- route_ids: int32 [64, 2], P('ep'), may hold values from 0 to 7, all different within a row; in each aligned block of 8 rows (0 to 7, 8 to 15, ...) at most 4 rows name the same one
- route_weights: float32 [64, 2], P('ep'), may hold values from 0.2 to 1
- expert_gate: bfloat16 [8, 2048, 2560], P('ep', None, 'tp'), may hold values from -0.125 to 0.125
- expert_up: bfloat16 [8, 2048, 2560], P('ep', None, 'tp'), may hold values from -0.125 to 0.125
- expert_down: bfloat16 [8, 2560, 2048], P('ep', 'tp'), may hold values from -0.15625 to 0.15625
- side_gate: bfloat16 [2048, 1024], P(None, 'tp'), may hold values from -0.125 to 0.125
- side_up: bfloat16 [2048, 1024], P(None, 'tp'), may hold values from -0.125 to 0.125
- side_down: bfloat16 [1024, 2048], P('tp'), may hold values from -0.25 to 0.25
- branch_gate: float32 [2048], replicated, may hold values from -0.125 to 0.125
Outputs:
- mixed: bfloat16 [64, 2048], P('ep', 'tp')
- new_keys: bfloat16 [64, 4096], P('ep', 'tp')
- new_values: bfloat16 [64, 4096], P('ep', 'tp')
Inputs may be any that keep to these rules, and one draw needn't show every extreme that they name: `lengths`: at least an eighth of 512; the first sequence has 512. `route_ids`: each token names 2 different experts. In the rows of one device no expert is named by more than 4 rows, a bound that some block reaches of some device.
All inputs are finite; a program needn't handle non-finite values.
Results may differ from a plain program's by a relative error of at most 0.018.
Values may be sent and summed in bfloat16 or wider, within the bound.
A program may use at most 64 MiB of HBM per device.

v0:
```python
import jax
import jax.numpy as jnp
from jax import lax
from jax.experimental import pallas as pl
from jax.experimental.pallas import tpu as pltpu
from jax.sharding import PartitionSpec as P

DH = 128


epsilon = 1e-06


def rms_scale(values, scale_gain):
    mean_square = jnp.mean(values * values, axis=-1, keepdims=True)
    return values * lax.rsqrt(mean_square + epsilon) * scale_gain


def body(
    tokens,
    attn_gain,
    query_weight,
    key_weight,
    value_weight,
    query_gain,
    stick_bias,
    key_cache,
    value_cache,
    lengths,
    out_weight,
    mix_gain,
    route_ids,
    route_weights,
    expert_gate,
    expert_up,
    expert_down,
    side_gate,
    side_up,
    side_down,
    branch_gate,
):
    seq_count, model_width = tokens.shape
    head_cols = query_weight.shape[1]
    heads_local = key_cache.shape[1]
    cache_slots = key_cache.shape[2]
    stream = tokens.astype(jnp.float32)
    normed = rms_scale(stream, attn_gain).astype(jnp.bfloat16)
    stacked = jnp.concatenate([query_weight, key_weight, value_weight], axis=1)
    columns = lax.all_to_all(normed, "ep", split_axis=1, concat_axis=0, tiled=True)
    picked = columns
    projected = lax.psum_scatter(
        jnp.dot(picked, stacked, preferred_element_type=jnp.float32),
        "ep",
        scatter_dimension=0,
        tiled=True,
    )
    query_rows = projected[:, :head_cols].astype(jnp.bfloat16)
    fresh_keys = projected[:, head_cols : 2 * head_cols].astype(jnp.bfloat16)
    new_values = projected[:, 2 * head_cols :].astype(jnp.bfloat16)
    new_keys = rms_scale(fresh_keys.astype(jnp.float32).reshape(seq_count, heads_local, DH), 1.0)
    new_keys = new_keys.astype(jnp.bfloat16).reshape(seq_count, head_cols)
    query_heads = rms_scale(
        query_rows.astype(jnp.float32).reshape(seq_count, heads_local, DH), query_gain
    )
    query_heads = query_heads.astype(jnp.bfloat16)
    scores = jnp.einsum("shd,shld->shl", query_heads, key_cache, preferred_element_type=jnp.float32)
    scores = scores * DH ** (-0.5) + stick_bias[None, :, None]
    positions = jnp.arange(cache_slots, dtype=jnp.int32)
    visible = positions[None, None, :] < lengths[:, None, None]
    log_rest = jnp.where(visible, jax.nn.log_sigmoid(-scores), 0.0)
    log_between = lax.cumsum(log_rest, axis=2, reverse=True) - log_rest
    stick = jnp.where(visible, jnp.exp(jax.nn.log_sigmoid(scores) + log_between), 0.0).astype(
        jnp.bfloat16
    )
    attended = jnp.einsum("shl,shld->shd", stick, value_cache, preferred_element_type=jnp.float32)
    attended = attended.astype(jnp.bfloat16).reshape(seq_count, head_cols)
    attn_proj = lax.psum(
        jnp.dot(attended, out_weight, preferred_element_type=jnp.float32).astype(jnp.bfloat16), "tp"
    ).astype(jnp.float32)
    middle = (stream + attn_proj).astype(jnp.bfloat16)
    normed_mix = rms_scale(middle.astype(jnp.float32), mix_gain).astype(jnp.bfloat16)
    side_gate_pre = jnp.dot(normed_mix, side_gate, preferred_element_type=jnp.float32)
    side_up_pre = jnp.dot(normed_mix, side_up, preferred_element_type=jnp.float32)
    side_hidden = (jax.nn.silu(side_gate_pre) * side_up_pre).astype(jnp.bfloat16)
    side_term = jnp.dot(side_hidden, side_down, preferred_element_type=jnp.float32)
    switch = jax.nn.sigmoid(
        jnp.sum(normed_mix.astype(jnp.float32) * branch_gate, axis=1, keepdims=True)
    )
    experts = lax.axis_size("ep")
    top_count = route_ids.shape[1]
    capacity = max(2, 2 * top_count * seq_count // experts)
    flat_ids = route_ids.reshape(-1)
    onehot = (flat_ids[:, None] == jnp.arange(experts, dtype=jnp.int32)[None, :]).astype(jnp.int32)
    before = jnp.cumsum(onehot, axis=0) - onehot
    slot_index = jnp.sum(before * onehot, axis=1)
    target = flat_ids * capacity + slot_index
    route_map = (
        target[:, None] == jnp.arange(experts * capacity, dtype=jnp.int32)[None, :]
    ).astype(jnp.bfloat16)
    dispatch = jnp.sum(route_map.reshape(seq_count, top_count, experts * capacity), axis=1).T
    outbox = jnp.dot(dispatch, normed_mix, preferred_element_type=jnp.float32).astype(jnp.bfloat16)
    outbox = outbox.reshape(experts, capacity, model_width)
    col_width = model_width // lax.axis_size("tp")
    col_offset = lax.axis_index("tp") * col_width
    arrived = lax.all_to_all(outbox, "ep", split_axis=0, concat_axis=0, tiled=True)
    slot_rows = arrived.reshape(experts * capacity, model_width)
    gate_pre = jnp.dot(slot_rows, expert_gate[0], preferred_element_type=jnp.float32)
    up_pre = jnp.dot(slot_rows, expert_up[0], preferred_element_type=jnp.float32)
    hidden = (jax.nn.silu(gate_pre) * up_pre).astype(jnp.bfloat16)
    expert_term = jnp.dot(hidden, expert_down[0], preferred_element_type=jnp.float32)
    expert_part, side_part = (
        lax.psum_scatter(
            expert_term.astype(jnp.bfloat16), "tp", scatter_dimension=1, tiled=True
        ).astype(jnp.float32),
        lax.psum_scatter(
            side_term.astype(jnp.bfloat16), "tp", scatter_dimension=1, tiled=True
        ).astype(jnp.float32),
    )
    returned = lax.all_to_all(
        expert_part.astype(jnp.bfloat16).reshape(experts, capacity, col_width),
        "ep",
        split_axis=0,
        concat_axis=0,
        tiled=True,
    )
    picked = jnp.dot(
        route_map,
        returned.reshape(experts * capacity, col_width),
        preferred_element_type=jnp.float32,
    )
    routed = jnp.sum(
        route_weights[:, :, None] * picked.reshape(seq_count, top_count, col_width), axis=1
    )
    middle_cols = lax.dynamic_slice_in_dim(middle, col_offset, col_width, 1).astype(jnp.float32)
    mixed = (middle_cols + routed + switch * side_part).astype(jnp.bfloat16)
    return (mixed, new_keys, new_values)


MESH = pl.DeviceIdType.MESH
F32 = jnp.float32
BF16 = jnp.bfloat16


def softplus(values):
    return jnp.maximum(values, 0.0) + jnp.log1p(jnp.exp(-jnp.abs(values)))


def silu(values):
    return values / (1.0 + jnp.exp(-values))


def as_columns(rows):
    count = rows.shape[1]
    own = lax.broadcasted_iota(jnp.int32, (count, count), 0) == lax.broadcasted_iota(
        jnp.int32, (count, count), 1
    )
    rows = rows.astype(F32)
    return [
        jnp.sum(jnp.where(own, rows[i : i + 1], 0.0), axis=1, keepdims=True)
        for i in range(rows.shape[0])
    ]


class Phases:
    def __init__(self):
        self.scope = None

    def __call__(self, name):
        if self.scope is not None:
            self.scope.__exit__(None, None, None)
        self.scope = jax.named_scope(name) if name else None
        if self.scope is not None:
            self.scope.__enter__()


def stack_rows(buffer):
    return jnp.concatenate([buffer[i].astype(F32) for i in range(buffer.shape[0])], axis=0)


def layer_kernel(
    n,
    m,
    tokens_ref,
    attn_gain_ref,
    query_gain_ref,
    bias_ref,
    lengths_ref,
    mix_gain_ref,
    ids_ref,
    weights_ref,
    branch_ref,
    wq_hbm,
    wk_hbm,
    wv_hbm,
    key_hbm,
    value_hbm,
    out_hbm,
    gate_hbm,
    up_hbm,
    down_hbm,
    side_gate_hbm,
    side_up_hbm,
    side_down_hbm,
    mixed_ref,
    new_keys_ref,
    new_values_ref,
    proj_w,
    keys,
    values,
    out_w,
    gate_w,
    up_w,
    down_w,
    side_gate_w,
    side_up_w,
    side_down_w,
    col_send,
    col_recv,
    query_send,
    query_recv,
    proj_send,
    proj_recv,
    head_rows,
    att_rows,
    reduce_buf,
    mid_cols,
    mix_send,
    mix_recv,
    slot_rows,
    slot_cols,
    side_cols,
    part_send,
    part_recv,
    back_send,
    back_recv,
    w_sem,
    k_sem,
    v_sem,
    o_sem,
    e_sem,
    ep_ss,
    ep_rs,
    tp_ss,
    tp_rs,
):
    ep = lax.axis_index("ep")
    tp = lax.axis_index("tp")
    seqs, width = tokens_ref.shape
    heads = keys.shape[1]
    slots = keys.shape[2]
    dh = keys.shape[3]
    cols = width // n
    out_cols = width // m

    loads = []

    def load(src, dst, sem):
        copy = pltpu.make_async_copy(src, dst, sem)
        copy.start()
        return copy

    proj_loads = [load(w, proj_w.at[i], w_sem.at[i]) for i, w in enumerate((wq_hbm, wk_hbm, wv_hbm))]
    key_loads = [load(key_hbm.at[i], keys.at[i], k_sem.at[i]) for i in range(seqs)]
    value_loads = [load(value_hbm.at[i], values.at[i], v_sem.at[i]) for i in range(seqs)]
    out_load = load(out_hbm, out_w, o_sem.at[0])
    side_loads = [
        load(side_gate_hbm, side_gate_w, o_sem.at[1]),
        load(side_up_hbm, side_up_w, o_sem.at[2]),
        load(side_down_hbm, side_down_w, o_sem.at[3]),
    ]
    expert_loads = [
        load(gate_hbm.at[0], gate_w, e_sem.at[0]),
        load(up_hbm.at[0], up_w, e_sem.at[1]),
        load(down_hbm.at[0], down_w, e_sem.at[2]),
    ]

    phase_name = Phases()
    phase_name("greet")
    barrier = pltpu.get_barrier_semaphore()
    for d in range(1, n):
        pl.semaphore_signal(barrier, inc=1, device_id=(lax.rem(ep + d, n), tp), device_id_type=MESH)
    for d in range(1, m):
        pl.semaphore_signal(barrier, inc=1, device_id=(ep, lax.rem(tp + d, m)), device_id_type=MESH)

    sent = []

    def ep_copy(phase, d, src, dst):
        return pltpu.make_async_remote_copy(
            src_ref=src,
            dst_ref=dst,
            send_sem=ep_ss.at[phase, d - 1],
            recv_sem=ep_rs.at[phase, d - 1],
            device_id=(lax.rem(ep + d, n), tp),
            device_id_type=MESH,
        )

    def tp_copy(phase, d, src, dst):
        return pltpu.make_async_remote_copy(
            src_ref=src,
            dst_ref=dst,
            send_sem=tp_ss.at[phase, d - 1],
            recv_sem=tp_rs.at[phase, d - 1],
            device_id=(ep, lax.rem(tp + d, m)),
            device_id_type=MESH,
        )

    def ep_scatter(phase, send, recv):
        for d in range(1, n):
            copy = ep_copy(phase, d, send.at[lax.rem(ep + d, n)], recv.at[ep])
            copy.start()
            sent.append(copy)

    def ep_arrive(phase, send, recv):
        for d in range(1, n):
            ep_copy(phase, d, send.at[0], recv.at[lax.rem(ep + n - d, n)]).wait_recv()

    stream = tokens_ref[...].astype(F32)
    normed = rms_scale(stream, attn_gain_ref[...])
    for j in range(n):
        col_send[j] = normed[:, j * cols : (j + 1) * cols].astype(BF16)
    col_recv[ep] = col_send[ep]
    phase_name("barrier")
    pl.semaphore_wait(barrier, (n - 1) + (m - 1))
    phase_name("col_send")
    ep_scatter(0, col_send, col_recv)

    later = lax.broadcasted_iota(jnp.int32, (slots, slots), 0) > lax.broadcasted_iota(
        jnp.int32, (slots, slots), 1
    )
    later = jnp.where(later, 1.0, 0.0).astype(BF16)
    capacity = mix_send.shape[1]
    lane_expert = lax.broadcasted_iota(jnp.int32, (seqs, n), 1).astype(F32)
    lane_slot = lax.broadcasted_iota(jnp.int32, (seqs, n * capacity), 1).astype(F32)
    row_slot = lax.broadcasted_iota(jnp.int32, (n * capacity, seqs), 0).astype(F32)
    first = lax.broadcasted_iota(jnp.int32, (seqs, seqs), 0)
    second = lax.broadcasted_iota(jnp.int32, (seqs, seqs), 1)
    weights = as_columns(weights_ref[...])
    ids = as_columns(ids_ref[...])
    named = [jnp.where(lane_expert == i, 1.0, 0.0) for i in ids]
    before = jnp.dot(
        jnp.where(second < first, 1.0, 0.0).astype(BF16),
        sum(named).astype(BF16),
        preferred_element_type=F32,
    )
    targets = [
        i * float(capacity) + jnp.sum(before * x, axis=1, keepdims=True) for i, x in zip(ids, named)
    ]
    route_map = jnp.concatenate(
        [jnp.where(lane_slot == t, 1.0, 0.0) for t in targets], axis=0
    ).astype(BF16)
    dispatch = sum(
        jnp.where(
            row_slot == jnp.sum(jnp.where(first == second, t, 0.0), axis=0, keepdims=True), 1.0, 0.0
        )
        for t in targets
    ).astype(BF16)
    phase_name("col_wait")
    ep_arrive(0, col_send, col_recv)
    phase_name("project")
    picked = stack_rows(col_recv).astype(BF16)

    half = query_send.shape[3]
    proj_loads[0].wait()
    for g in range(2):
        part = jnp.dot(
            picked, proj_w[0, :, g * half : (g + 1) * half], preferred_element_type=F32
        )
        for j in range(n):
            query_send[g, j] = part[j * seqs : (j + 1) * seqs].astype(BF16)
        query_recv[g, ep] = query_send[g, ep]
        ep_scatter(1 if g == 0 else 5 + m, query_send.at[g], query_recv.at[g])
    for i in (1, 2):
        proj_loads[i].wait()
        part = jnp.dot(picked, proj_w[i], preferred_element_type=F32)
        for j in range(n):
            proj_send[i - 1, j] = part[j * seqs : (j + 1) * seqs].astype(BF16)
        proj_recv[i - 1, ep] = proj_send[i - 1, ep]
    head_rows[...] = jnp.zeros_like(head_rows)

    def collect(phase, send, recv):
        ep_arrive(phase, send, recv)
        total = recv[0].astype(F32)
        for j in range(1, n):
            total = total + recv[j].astype(F32)
        return total.astype(BF16).astype(F32)

    row = lax.broadcasted_iota(jnp.int32, (heads, slots), 0)
    position = lax.broadcasted_iota(jnp.int32, (heads, slots), 1)
    bias = as_columns(bias_ref[...])[0]
    lengths = as_columns(lengths_ref[...])[0].astype(jnp.int32)
    scale = dh ** (-0.5)
    every_rows = [jnp.zeros((heads, slots), F32)] * seqs
    some = half // dh
    for g in range(2):
        phase_name("query_wait")
        query = collect(1 if g == 0 else 5 + m, query_send.at[g], query_recv.at[g])
        phase_name("scores")
        if g == 0:
            for i in range(2):
                ep_scatter(2 + i, proj_send.at[i], proj_recv.at[i])
        for h in range(some):
            head_rows[pl.ds(g * some + h, seqs, stride=heads), :] = rms_scale(
                query[:, h * dh : (h + 1) * dh], query_gain_ref[...]
            )
        for s in range(seqs):
            if g == 0:
                key_loads[s].wait()
            q = head_rows[s * heads : (s + 1) * heads, :].astype(BF16)
            each = lax.dot_general(
                q,
                keys[s, g * some : (g + 1) * some].reshape(some * slots, dh),
                (((1,), (1,)), ((), ())),
                preferred_element_type=F32,
            )
            for h in range(some):
                every_rows[s] = jnp.where(
                    row == g * some + h, each[:, h * slots : (h + 1) * slots], every_rows[s]
                )
    every = jnp.concatenate(every_rows, axis=0)
    score_rows, rest_rows, seen = [], [], []
    for s in range(seqs):
        score = every[s * heads : (s + 1) * heads] * scale + bias
        visible = position < lengths[s : s + 1]
        full = -softplus(score)
        seen.append(visible)
        score_rows.append(score + full)
        rest_rows.append(jnp.where(visible, full, 0.0))
    phase_name("between")
    rest = jnp.concatenate(rest_rows, axis=0)
    high = rest.astype(BF16)
    left = rest - high.astype(F32)
    middle_part = left.astype(BF16)
    low = (left - middle_part.astype(F32)).astype(BF16)
    between = (
        jnp.dot(high, later, preferred_element_type=F32)
        + jnp.dot(middle_part, later, preferred_element_type=F32)
        + jnp.dot(low, later, preferred_element_type=F32)
    )
    phase_name("attend")
    for s in range(seqs):
        value_loads[s].wait()
        stick = jnp.where(
            seen[s], jnp.exp(score_rows[s] + between[s * heads : (s + 1) * heads]), 0.0
        )
        spread = jnp.concatenate(
            [jnp.where(row == h, stick, 0.0).astype(BF16) for h in range(heads)], axis=1
        )
        att_rows[s * heads : (s + 1) * heads, :] = jnp.dot(
            spread, values[s].reshape(heads * slots, dh), preferred_element_type=F32
        )
    phase_name("out_proj")
    attended = jnp.concatenate(
        [att_rows[pl.ds(h, seqs, stride=heads), :] for h in range(heads)], axis=1
    ).astype(BF16)
    out_load.wait()
    for t in range(m):
        reduce_buf[t, tp] = jnp.dot(
            attended, out_w[:, t * out_cols : (t + 1) * out_cols], preferred_element_type=F32
        ).astype(BF16)
        for d in range(1, m):
            copy = tp_copy(t, d, reduce_buf.at[t, tp], reduce_buf.at[t, tp])
            copy.start()
            sent.append(copy)

    phase_name("reduce_wait")
    projected = []
    for t in range(m):
        for d in range(1, m):
            source = lax.rem(tp + m - d, m)
            tp_copy(t, d, reduce_buf.at[t, tp], reduce_buf.at[t, source]).wait_recv()
        projected.append(sum(reduce_buf[t, i].astype(F32) for i in range(m)))
    phase_name("mix")
    middle = (stream + jnp.concatenate(projected, axis=1)).astype(BF16).astype(F32)
    for t in range(m):
        mid_cols[t] = middle[:, t * out_cols : (t + 1) * out_cols]
    normed_mix = rms_scale(middle, mix_gain_ref[...]).astype(BF16)
    outbox = jnp.dot(dispatch, normed_mix, preferred_element_type=F32)
    for j in range(n):
        mix_send[j] = outbox[j * capacity : (j + 1) * capacity].astype(BF16)
    mix_recv[ep] = mix_send[ep]
    ep_scatter(4, mix_send, mix_recv)

    phase_name("side")
    for copy in side_loads:
        copy.wait()
    side_hidden = silu(
        jnp.dot(normed_mix, side_gate_w[...], preferred_element_type=F32)
    ) * jnp.dot(normed_mix, side_up_w[...], preferred_element_type=F32)
    side_term = jnp.dot(side_hidden.astype(BF16), side_down_w[...], preferred_element_type=F32)
    switch = jnp.sum(normed_mix.astype(F32) * branch_ref[...], axis=1, keepdims=True)
    switch = 1.0 / (1.0 + jnp.exp(-switch))

    phase_name("new_keys")
    key_rows = collect(2, proj_send.at[0], proj_recv.at[0])
    for h in range(heads):
        part = slice(h * dh, (h + 1) * dh)
        new_keys_ref[:, part] = rms_scale(key_rows[:, part], 1.0).astype(BF16)
    new_values_ref[...] = collect(3, proj_send.at[1], proj_recv.at[1]).astype(BF16)

    phase_name("rows_wait")
    for copy in expert_loads:
        copy.wait()
    ep_arrive(4, mix_send, mix_recv)
    phase_name("expert")
    for j in range(n):
        slot_rows[j * capacity : (j + 1) * capacity, :] = mix_recv[j].astype(F32)
    rows = slot_rows[...].astype(BF16)
    hidden = silu(jnp.dot(rows, gate_w[...], preferred_element_type=F32)) * jnp.dot(
        rows, up_w[...], preferred_element_type=F32
    )
    hidden = hidden.astype(BF16)
    order = [lax.rem(tp + d, m) for d in (*range(1, m), 0)]
    for i, t in enumerate(order):
        columns = pl.ds(pl.multiple_of(t * out_cols, out_cols), out_cols)
        expert_term = jnp.dot(hidden, down_w[:, columns], preferred_element_type=F32)
        for j in range(n):
            back_send[i, j] = expert_term[j * capacity : (j + 1) * capacity].astype(BF16)
        back_recv[i, ep] = back_send[i, ep]
        ep_scatter(5 + i, back_send.at[i], back_recv.at[i])
    for t in range(m):
        side_cols[t] = switch * side_term[:, t * out_cols : (t + 1) * out_cols]
    for i, t in enumerate(order):
        phase_name("back_wait")
        ep_arrive(5 + i, back_send.at[i], back_recv.at[i])
        phase_name("combine")
        for j in range(n):
            slot_cols[j * capacity : (j + 1) * capacity, :] = back_recv[i, j].astype(F32)
        chosen = jnp.dot(route_map, slot_cols[...].astype(BF16), preferred_element_type=F32)
        share = side_cols[t]
        for k, w in enumerate(weights):
            share = share + w * chosen[k * seqs : (k + 1) * seqs]
        if i < m - 1:
            part_send[i] = share.astype(BF16)
            copy = tp_copy(m, i + 1, part_send.at[i], part_recv.at[i])
            copy.start()
            sent.append(copy)
    result = mid_cols[tp] + share
    phase_name("part_wait")
    for d in range(1, m):
        tp_copy(m, d, part_send.at[d - 1], part_recv.at[d - 1]).wait_recv()
        result = result + part_recv[d - 1].astype(F32)
    mixed_ref[...] = result.astype(BF16)
    phase_name("drain")
    for copy in sent:
        copy.wait_send()
    phase_name(None)


def hand_on(*refs):
    count = len(refs) // 2
    for src, dst in zip(refs[:count], refs[count:]):
        dst[...] = src[...]


def fused(n, m, *args):
    (
        tokens,
        attn_gain,
        query_weight,
        key_weight,
        value_weight,
        query_gain,
        stick_bias,
        key_cache,
        value_cache,
        lengths,
        out_weight,
        mix_gain,
        route_ids,
        route_weights,
        expert_gate,
        expert_up,
        expert_down,
        side_gate,
        side_up,
        side_down,
        branch_gate,
    ) = args
    seqs, width = tokens.shape
    _, heads, slots, dh = key_cache.shape
    head_cols = query_weight.shape[1]
    out_cols = width // m
    capacity = max(2, 2 * route_ids.shape[1] * seqs // n)
    vmem = pl.BlockSpec(memory_space=pltpu.VMEM)
    hbm = pl.BlockSpec(memory_space=pl.ANY)
    dma = pltpu.SemaphoreType.DMA

    def scratch(*shape, dtype=BF16):
        return pltpu.VMEM(shape, dtype)

    outs = pl.pallas_call(
        lambda *refs: layer_kernel(n, m, *refs),
        out_shape=(
            jax.ShapeDtypeStruct((seqs, out_cols), BF16),
            jax.ShapeDtypeStruct((seqs, head_cols), BF16),
            jax.ShapeDtypeStruct((seqs, head_cols), BF16),
        ),
        in_specs=[vmem] * 9 + [hbm] * 12,
        out_specs=(vmem, vmem, vmem),
        scratch_shapes=[
            scratch(3, *query_weight.shape),
            scratch(*key_cache.shape),
            scratch(*value_cache.shape),
            scratch(*out_weight.shape),
            scratch(*expert_gate.shape[1:]),
            scratch(*expert_up.shape[1:]),
            scratch(*expert_down.shape[1:]),
            scratch(*side_gate.shape),
            scratch(*side_up.shape),
            scratch(*side_down.shape),
            scratch(n, seqs, width // n),
            scratch(n, seqs, width // n),
            scratch(2, n, seqs, head_cols // 2),
            scratch(2, n, seqs, head_cols // 2),
            scratch(2, n, seqs, head_cols),
            scratch(2, n, seqs, head_cols),
            scratch(-(-seqs * heads // 128) * 128, dh, dtype=F32),
            scratch(seqs * heads, dh, dtype=F32),
            scratch(m, m, seqs, out_cols),
            scratch(m, seqs, out_cols, dtype=F32),
            scratch(n, capacity, width),
            scratch(n, capacity, width),
            scratch(n * capacity, width, dtype=F32),
            scratch(n * capacity, out_cols, dtype=F32),
            scratch(m, seqs, out_cols, dtype=F32),
            scratch(m - 1, seqs, out_cols),
            scratch(m - 1, seqs, out_cols),
            scratch(m, n, capacity, out_cols),
            scratch(m, n, capacity, out_cols),
            dma((3,)),
            dma((seqs,)),
            dma((seqs,)),
            dma((4,)),
            dma((3,)),
            dma((6 + m, n - 1)),
            dma((6 + m, n - 1)),
            dma((m + 1, m - 1)),
            dma((m + 1, m - 1)),
        ],
        compiler_params=pltpu.CompilerParams(
            collective_id=0, has_side_effects=True, vmem_limit_bytes=60 * 1024 * 1024
        ),
        name="layer",
    )(
        tokens,
        attn_gain.reshape(1, width),
        query_gain.reshape(1, dh),
        stick_bias.reshape(1, heads),
        lengths.reshape(1, seqs),
        mix_gain.reshape(1, width),
        route_ids.T,
        route_weights.T,
        branch_gate.reshape(1, width),
        query_weight,
        key_weight,
        value_weight,
        key_cache,
        value_cache,
        out_weight,
        expert_gate,
        expert_up,
        expert_down,
        side_gate,
        side_up,
        side_down,
    )
    return pl.pallas_call(
        hand_on,
        out_shape=tuple(jax.ShapeDtypeStruct(x.shape, x.dtype) for x in outs),
        in_specs=[vmem] * len(outs),
        out_specs=(vmem,) * len(outs),
        name="hand_on",
    )(*outs)


def layer(n, m, *args):
    tokens, query_weight, key_cache = args[0], args[2], args[7]
    expert_gate, side_gate = args[14], args[17]
    seqs, width = tokens.shape
    lanes = (width // n, width // m, query_weight.shape[1], key_cache.shape[2])
    lanes += (key_cache.shape[3], expert_gate.shape[2], side_gate.shape[1])
    lanes += (query_weight.shape[1] // 2,)
    rows = (seqs, key_cache.shape[1])
    held = 2 * sum(a.size for a in args[2:] if a.dtype == BF16)
    aligned = all(x % 128 == 0 for x in lanes) and all(x % 8 == 0 for x in rows)
    if n > 1 and m > 1 and aligned and expert_gate.shape[0] == 1 and held < 48 * 1024 * 1024:
        return fused(n, m, *args)
    return body(*args)


def solution(mesh):
    in_specs = (
        P("ep", None),
        P(),
        P("ep", "tp"),
        P("ep", "tp"),
        P("ep", "tp"),
        P(),
        P("tp"),
        P("ep", "tp", None, None),
        P("ep", "tp", None, None),
        P("ep"),
        P("tp", None),
        P(),
        P("ep", None),
        P("ep", None),
        P("ep", None, "tp"),
        P("ep", None, "tp"),
        P("ep", "tp", None),
        P(None, "tp"),
        P(None, "tp"),
        P("tp", None),
        P(),
    )
    out_specs = (P("ep", "tp"), P("ep", "tp"), P("ep", "tp"))
    return jax.shard_map(
        lambda *args: layer(mesh.shape["ep"], mesh.shape["tp"], *args),
        mesh=mesh,
        in_specs=in_specs,
        out_specs=out_specs,
        check_vma=False,
    )
```

profile of v0, /device:TPU:0, one launch (start us, length us, event | category | flops | bytes accessed | tf_op | source)
XLA Modules:
  0.0 42.0 jit_solution(16863529004023427621)
XLA Ops:
  0.6 40.0 %layer.1 = (bf16[8,512]{1,0:T(8,128)(2,1)}, bf16[8,1024]{1,0:T(8,128)(2,1)}, bf16[8,1024]{1,0:T(8,128)(2,1)}) custom-call(bf16[8,2048]{1,0:T(8,128)(2,1)} %refs_0_.1, f32[1,2048]{1,0:T(1,128)} %bitcast.8, f32[1,128]{1,0:T(1,128)} %bitcast.13, f32[1,8]{1,0:T(1,128)} %bitcast.14, s32[1,8]{1,0:T(1,128)} %bitcast.15, f32[1,2048]{1,0:T(1,128)} %bitcast.9, ...), custom_call_target="tpu_custom_call" | custom-call | tf_op jit(solution)/shard_map/layer/pallas_call | solution.py:591
  40.6 1.4 %hand_on.1 = (bf16[8,512]{1,0:T(8,128)(2,1)}, bf16[8,1024]{1,0:T(8,128)(2,1)}, bf16[8,1024]{1,0:T(8,128)(2,1)}) custom-call(bf16[8,512]{1,0:T(8,128)(2,1)} %get-tuple-element.6.refs_0_, bf16[8,1024]{1,0:T(8,128)(2,1)} %get-tuple-element.7.refs_1_, bf16[8,1024]{1,0:T(8,128)(2,1)} %get-tuple-element.8.refs_2_), custom_call_target="tpu_custom_call" | custom-call | tf_op jit(solution)/shard_map/hand_on/pallas_call | solution.py:667
where the time goes:
time: 42.2 us; the launch traced here: 42 us
  Pallas kernels  41.3 us (98%)
  between operations  0.65 us (2%)
    pallas_call x1, Pallas kernels, fused(): pl.pallas_call(lambda *refs: layer_kernel(n, m, *refs), out_shape=(jax.Sh...  40 us
    pallas_call x1, Pallas kernels, fused(): pl.pallas_call(hand_on, out_shape=tuple((jax.ShapeDtypeStruct(x.shape, x....  1.37 us

commit v1 on v0

v1 whole, which is shorter than its diff:
```python
import jax
import jax.numpy as jnp
from jax import lax
from jax.experimental import pallas as pl
from jax.experimental.pallas import tpu as pltpu
from jax.sharding import PartitionSpec as P

DH = 128


epsilon = 1e-06


def rms_scale(values, scale_gain):
    mean_square = jnp.mean(values * values, axis=-1, keepdims=True)
    return values * lax.rsqrt(mean_square + epsilon) * scale_gain


def body(
    tokens,
    attn_gain,
    query_weight,
    key_weight,
    value_weight,
    query_gain,
    stick_bias,
    key_cache,
    value_cache,
    lengths,
    out_weight,
    mix_gain,
    route_ids,
    route_weights,
    expert_gate,
    expert_up,
    expert_down,
    side_gate,
    side_up,
    side_down,
    branch_gate,
):
    seq_count, model_width = tokens.shape
    head_cols = query_weight.shape[1]
    heads_local = key_cache.shape[1]
    cache_slots = key_cache.shape[2]
    stream = tokens.astype(jnp.float32)
    normed = rms_scale(stream, attn_gain).astype(jnp.bfloat16)
    stacked = jnp.concatenate([query_weight, key_weight, value_weight], axis=1)
    columns = lax.all_to_all(normed, "ep", split_axis=1, concat_axis=0, tiled=True)
    picked = columns
    projected = lax.psum_scatter(
        jnp.dot(picked, stacked, preferred_element_type=jnp.float32),
        "ep",
        scatter_dimension=0,
        tiled=True,
    )
    query_rows = projected[:, :head_cols].astype(jnp.bfloat16)
    fresh_keys = projected[:, head_cols : 2 * head_cols].astype(jnp.bfloat16)
    new_values = projected[:, 2 * head_cols :].astype(jnp.bfloat16)
    new_keys = rms_scale(fresh_keys.astype(jnp.float32).reshape(seq_count, heads_local, DH), 1.0)
    new_keys = new_keys.astype(jnp.bfloat16).reshape(seq_count, head_cols)
    query_heads = rms_scale(
        query_rows.astype(jnp.float32).reshape(seq_count, heads_local, DH), query_gain
    )
    query_heads = query_heads.astype(jnp.bfloat16)
    scores = jnp.einsum("shd,shld->shl", query_heads, key_cache, preferred_element_type=jnp.float32)
    scores = scores * DH ** (-0.5) + stick_bias[None, :, None]
    positions = jnp.arange(cache_slots, dtype=jnp.int32)
    visible = positions[None, None, :] < lengths[:, None, None]
    log_rest = jnp.where(visible, jax.nn.log_sigmoid(-scores), 0.0)
    log_between = lax.cumsum(log_rest, axis=2, reverse=True) - log_rest
    stick = jnp.where(visible, jnp.exp(jax.nn.log_sigmoid(scores) + log_between), 0.0).astype(
        jnp.bfloat16
    )
    attended = jnp.einsum("shl,shld->shd", stick, value_cache, preferred_element_type=jnp.float32)
    attended = attended.astype(jnp.bfloat16).reshape(seq_count, head_cols)
    attn_proj = lax.psum(
        jnp.dot(attended, out_weight, preferred_element_type=jnp.float32).astype(jnp.bfloat16), "tp"
    ).astype(jnp.float32)
    middle = (stream + attn_proj).astype(jnp.bfloat16)
    normed_mix = rms_scale(middle.astype(jnp.float32), mix_gain).astype(jnp.bfloat16)
    side_gate_pre = jnp.dot(normed_mix, side_gate, preferred_element_type=jnp.float32)
    side_up_pre = jnp.dot(normed_mix, side_up, preferred_element_type=jnp.float32)
    side_hidden = (jax.nn.silu(side_gate_pre) * side_up_pre).astype(jnp.bfloat16)
    side_term = jnp.dot(side_hidden, side_down, preferred_element_type=jnp.float32)
    switch = jax.nn.sigmoid(
        jnp.sum(normed_mix.astype(jnp.float32) * branch_gate, axis=1, keepdims=True)
    )
    experts = lax.axis_size("ep")
    top_count = route_ids.shape[1]
    capacity = max(2, 2 * top_count * seq_count // experts)
    flat_ids = route_ids.reshape(-1)
    onehot = (flat_ids[:, None] == jnp.arange(experts, dtype=jnp.int32)[None, :]).astype(jnp.int32)
    before = jnp.cumsum(onehot, axis=0) - onehot
    slot_index = jnp.sum(before * onehot, axis=1)
    target = flat_ids * capacity + slot_index
    route_map = (
        target[:, None] == jnp.arange(experts * capacity, dtype=jnp.int32)[None, :]
    ).astype(jnp.bfloat16)
    dispatch = jnp.sum(route_map.reshape(seq_count, top_count, experts * capacity), axis=1).T
    outbox = jnp.dot(dispatch, normed_mix, preferred_element_type=jnp.float32).astype(jnp.bfloat16)
    outbox = outbox.reshape(experts, capacity, model_width)
    col_width = model_width // lax.axis_size("tp")
    col_offset = lax.axis_index("tp") * col_width
    arrived = lax.all_to_all(outbox, "ep", split_axis=0, concat_axis=0, tiled=True)
    slot_rows = arrived.reshape(experts * capacity, model_width)
    gate_pre = jnp.dot(slot_rows, expert_gate[0], preferred_element_type=jnp.float32)
    up_pre = jnp.dot(slot_rows, expert_up[0], preferred_element_type=jnp.float32)
    hidden = (jax.nn.silu(gate_pre) * up_pre).astype(jnp.bfloat16)
    expert_term = jnp.dot(hidden, expert_down[0], preferred_element_type=jnp.float32)
    expert_part, side_part = (
        lax.psum_scatter(
            expert_term.astype(jnp.bfloat16), "tp", scatter_dimension=1, tiled=True
        ).astype(jnp.float32),
        lax.psum_scatter(
            side_term.astype(jnp.bfloat16), "tp", scatter_dimension=1, tiled=True
        ).astype(jnp.float32),
    )
    returned = lax.all_to_all(
        expert_part.astype(jnp.bfloat16).reshape(experts, capacity, col_width),
        "ep",
        split_axis=0,
        concat_axis=0,
        tiled=True,
    )
    picked = jnp.dot(
        route_map,
        returned.reshape(experts * capacity, col_width),
        preferred_element_type=jnp.float32,
    )
    routed = jnp.sum(
        route_weights[:, :, None] * picked.reshape(seq_count, top_count, col_width), axis=1
    )
    middle_cols = lax.dynamic_slice_in_dim(middle, col_offset, col_width, 1).astype(jnp.float32)
    mixed = (middle_cols + routed + switch * side_part).astype(jnp.bfloat16)
    return (mixed, new_keys, new_values)


MESH = pl.DeviceIdType.MESH
F32 = jnp.float32
BF16 = jnp.bfloat16


def softplus(values):
    return jnp.maximum(values, 0.0) + jnp.log1p(jnp.exp(-jnp.abs(values)))


def silu(values):
    return values / (1.0 + jnp.exp(-values))


def as_columns(rows):
    count = rows.shape[1]
    own = lax.broadcasted_iota(jnp.int32, (count, count), 0) == lax.broadcasted_iota(
        jnp.int32, (count, count), 1
    )
    rows = rows.astype(F32)
    return [
        jnp.sum(jnp.where(own, rows[i : i + 1], 0.0), axis=1, keepdims=True)
        for i in range(rows.shape[0])
    ]


class Phases:
    def __init__(self):
        self.scope = None

    def __call__(self, name):
        if self.scope is not None:
            self.scope.__exit__(None, None, None)
        self.scope = jax.named_scope(name) if name else None
        if self.scope is not None:
            self.scope.__enter__()


def stack_rows(buffer):
    return jnp.concatenate([buffer[i].astype(F32) for i in range(buffer.shape[0])], axis=0)


def layer_kernel(
    n,
    m,
    tokens_hbm,
    attn_gain_hbm,
    query_gain_hbm,
    bias_hbm,
    lengths_hbm,
    mix_gain_hbm,
    ids_hbm,
    weights_hbm,
    branch_hbm,
    wq_hbm,
    wk_hbm,
    wv_hbm,
    key_hbm,
    value_hbm,
    out_hbm,
    gate_hbm,
    up_hbm,
    down_hbm,
    side_gate_hbm,
    side_up_hbm,
    side_down_hbm,
    mixed_ref,
    new_keys_ref,
    new_values_ref,
    tokens_ref,
    rows_ref,
    query_gain_ref,
    bias_ref,
    lengths_ref,
    ids_ref,
    weights_ref,
    proj_w,
    keys,
    turned,
    values,
    out_w,
    expert_w,
    down_w,
    side_w,
    side_down_w,
    col_send,
    col_recv,
    query_send,
    query_recv,
    proj_send,
    proj_recv,
    reduce_buf,
    mid_cols,
    mix_send,
    mix_recv,
    slot_rows,
    slot_cols,
    side_cols,
    side_send,
    side_recv,
    back_send,
    back_recv,
    load_sem,
    send_sem,
    recv_sem,
):
    ep = lax.axis_index("ep")
    tp = lax.axis_index("tp")
    seqs, width = tokens_ref.shape
    heads, dh, slots = turned.shape[0], turned.shape[2], turned.shape[3]
    cols = width // n
    out_cols = width // m
    parts = reduce_buf.shape[0]
    part_cols = width // parts

    phase_name = Phases()
    phase_name("greet")
    barrier = pltpu.get_barrier_semaphore()
    for d in range(1, n):
        pl.semaphore_signal(barrier, inc=1, device_id=(lax.rem(ep + d, n), tp), device_id_type=MESH)
    for d in range(1, m):
        pl.semaphore_signal(barrier, inc=1, device_id=(ep, lax.rem(tp + d, m)), device_id_type=MESH)

    def load(k, whole, *pairs, priority=1):
        for src, dst in pairs:
            pltpu.make_async_copy(src, dst, load_sem.at[k]).start(priority=priority)
        return pltpu.make_async_copy(whole, whole, load_sem.at[k])

    tokens_load = load(0, tokens_ref, (tokens_hbm, tokens_ref), priority=0)
    gains = (attn_gain_hbm, mix_gain_hbm, branch_hbm)
    rows_load = load(1, rows_ref, *((x, rows_ref.at[i]) for i, x in enumerate(gains)), priority=0)
    small = (
        (ids_hbm, ids_ref),
        (weights_hbm, weights_ref),
        (query_gain_hbm, query_gain_ref),
        (bias_hbm, bias_ref),
        (lengths_hbm, lengths_ref),
    )
    small_loads = [load(2 + i, x[1], x, priority=0) for i, x in enumerate(small)]
    proj_load = load(
        7,
        proj_w,
        *((w, proj_w.at[i]) for i, w in enumerate((wq_hbm, wk_hbm, wv_hbm))),
        priority=0,
    )
    key_load = load(8, keys, *((key_hbm.at[i], keys.at[i]) for i in range(seqs)))
    value_load = load(9, values, *((value_hbm.at[i], values.at[:, i]) for i in range(seqs)))

    def remote(sem, src, dst, target, arrival=None):
        copy = pltpu.make_async_remote_copy(
            src_ref=src,
            dst_ref=dst,
            send_sem=send_sem.at[sem],
            recv_sem=recv_sem.at[sem if arrival is None else arrival],
            device_id=target,
            device_id_type=MESH,
        )
        copy.start()

    def sent(sem, whole):
        pltpu.make_async_copy(whole, whole, send_sem.at[sem]).wait()

    def arrived(sem, whole):
        pltpu.make_async_copy(whole, whole, recv_sem.at[sem]).wait()

    def ep_scatter(sem, send, recv, arrival=None):
        for d in range(1, n):
            j = lax.rem(ep + d, n)
            remote(sem, send.at[j], recv.at[ep], (j, tp), arrival)

    others = pl.ds(0, n - 1)
    fellows = pl.ds(0, m - 1)
    s_col, s_query, s_proj, s_reduce, s_mix, s_side, s_back, s_near = range(8)
    r_query, r_reduce, r_mix = 8, 10, 10 + parts

    tokens_load.wait()
    rows_load.wait()
    attn_gain, mix_gain, branch_gate = (rows_ref[i] for i in range(3))
    stream = tokens_ref[...].astype(F32)
    normed = rms_scale(stream, attn_gain)
    for j in range(n):
        col_send[j] = normed[:, j * cols : (j + 1) * cols].astype(BF16)
    col_recv[ep] = col_send[ep]
    phase_name("barrier")
    pl.semaphore_wait(barrier, (n - 1) + (m - 1))
    phase_name("col_send")
    ep_scatter(s_col, col_send, col_recv)

    for copy in small_loads:
        copy.wait()
    later = lax.broadcasted_iota(jnp.int32, (slots, slots), 0) > lax.broadcasted_iota(
        jnp.int32, (slots, slots), 1
    )
    later = jnp.where(later, 1.0, 0.0).astype(BF16)
    capacity = mix_send.shape[2]
    lane_expert = lax.broadcasted_iota(jnp.int32, (seqs, n), 1).astype(F32)
    lane_slot = lax.broadcasted_iota(jnp.int32, (seqs, n * capacity), 1).astype(F32)
    row_slot = lax.broadcasted_iota(jnp.int32, (n * capacity, seqs), 0).astype(F32)
    first = lax.broadcasted_iota(jnp.int32, (seqs, seqs), 0)
    second = lax.broadcasted_iota(jnp.int32, (seqs, seqs), 1)
    weights = as_columns(weights_ref[...])
    ids = as_columns(ids_ref[...])
    named = [jnp.where(lane_expert == i, 1.0, 0.0) for i in ids]
    before = jnp.dot(
        jnp.where(second < first, 1.0, 0.0).astype(BF16),
        sum(named).astype(BF16),
        preferred_element_type=F32,
    )
    targets = [
        i * float(capacity) + jnp.sum(before * x, axis=1, keepdims=True) for i, x in zip(ids, named)
    ]
    route_map = jnp.concatenate(
        [jnp.where(lane_slot == t, 1.0, 0.0) for t in targets], axis=0
    ).astype(BF16)
    dispatch = sum(
        jnp.where(
            row_slot == jnp.sum(jnp.where(first == second, t, 0.0), axis=0, keepdims=True), 1.0, 0.0
        )
        for t in targets
    ).astype(BF16)
    proj_load.wait()
    phase_name("col_wait")
    arrived(s_col, col_recv.at[others])
    phase_name("project")
    picked = stack_rows(col_recv).astype(BF16)

    half = query_send.shape[3]
    for g in range(2):
        part = jnp.dot(
            picked, proj_w[0, :, g * half : (g + 1) * half], preferred_element_type=F32
        )
        for j in range(n):
            query_send[g, j] = part[j * seqs : (j + 1) * seqs].astype(BF16)
        query_recv[g, ep] = query_send[g, ep]
        ep_scatter(s_query, query_send.at[g], query_recv.at[g], r_query + g)
    phase_name("turn")
    out_load = load(10, out_w, (out_hbm, out_w))
    side_load = load(11, side_w, (side_gate_hbm, side_w.at[0]), (side_up_hbm, side_w.at[1]))
    side_down_load = load(12, side_down_w, (side_down_hbm, side_down_w))
    expert_load = load(13, expert_w, (gate_hbm.at[0], expert_w.at[0]), (up_hbm.at[0], expert_w.at[1]))
    down_load = load(14, down_w, (down_hbm.at[0], down_w))
    for i in (1, 2):
        part = jnp.dot(picked, proj_w[i], preferred_element_type=F32)
        for j in range(n):
            proj_send[i - 1, j] = part[j * seqs : (j + 1) * seqs].astype(BF16)
        proj_recv[i - 1, ep] = proj_send[i - 1, ep]
    key_load.wait()
    for s in range(seqs):
        for h in range(heads):
            turned[h, s] = keys[s, h].T
    value_load.wait()

    def collect(recv):
        total = recv[0].astype(F32)
        for j in range(1, n):
            total = total + recv[j].astype(F32)
        return total.astype(BF16).astype(F32)

    query_row = lax.broadcasted_iota(jnp.int32, (seqs, dh), 0)
    slot_row = lax.broadcasted_iota(jnp.int32, (seqs, slots), 0)
    position = lax.broadcasted_iota(jnp.int32, (seqs, slots), 1)
    lengths = as_columns(lengths_ref[...])[0].astype(jnp.int32)
    visible = position < lengths
    scale = dh ** (-0.5)
    some = half // dh
    score_rows, rest_rows = [], []
    for g in range(2):
        phase_name("query_wait")
        arrived(r_query + g, query_recv.at[g, others])
        phase_name("scores")
        query = collect(query_recv.at[g])
        if g == 0:
            for i in range(2):
                ep_scatter(s_proj, proj_send.at[i], proj_recv.at[i])
        for k in range(some):
            h = g * some + k
            q = rms_scale(query[:, k * dh : (k + 1) * dh], query_gain_ref[...])
            spread = jnp.concatenate(
                [jnp.where(query_row == s, q, 0.0).astype(BF16) for s in range(seqs)], axis=1
            )
            score = jnp.dot(
                spread, turned[h].reshape(seqs * dh, slots), preferred_element_type=F32
            )
            score = score * scale + bias_ref[0:1, h : h + 1]
            full = -softplus(score)
            score_rows.append(score + full)
            rest_rows.append(jnp.where(visible, full, 0.0))
    rest = jnp.concatenate(rest_rows, axis=0)
    high = rest.astype(BF16)
    left = rest - high.astype(F32)
    middle_part = left.astype(BF16)
    low = (left - middle_part.astype(F32)).astype(BF16)
    pieces = jnp.dot(
        jnp.concatenate([high, middle_part, low], axis=0), later, preferred_element_type=F32
    )
    count = seqs * heads
    between = pieces[:count] + pieces[count : 2 * count] + pieces[2 * count :]
    attended = []
    for h in range(heads):
        stick = jnp.where(
            visible, jnp.exp(score_rows[h] + between[h * seqs : (h + 1) * seqs]), 0.0
        )
        spread = jnp.concatenate(
            [jnp.where(slot_row == s, stick, 0.0).astype(BF16) for s in range(seqs)], axis=1
        )
        attended.append(
            jnp.dot(spread, values[h].reshape(seqs * slots, dh), preferred_element_type=F32)
        )
    attended = jnp.concatenate(attended, axis=1).astype(BF16)
    phase_name("out_proj")
    out_load.wait()
    for t in range(parts):
        reduce_buf[t, tp] = jnp.dot(
            attended, out_w[:, t * part_cols : (t + 1) * part_cols], preferred_element_type=F32
        ).astype(BF16)
        for d in range(1, m):
            own = reduce_buf.at[t, tp]
            remote(s_reduce, own, own, (ep, lax.rem(tp + d, m)), r_reduce + t)

    middle = []
    for t in range(parts):
        phase_name("reduce_wait")
        arrived(r_reduce + t, reduce_buf.at[t, fellows])
        phase_name("mix")
        total = sum(reduce_buf[t, i].astype(F32) for i in range(m))
        part = (stream[:, t * part_cols : (t + 1) * part_cols] + total).astype(BF16)
        outbox = jnp.dot(dispatch, part, preferred_element_type=F32)
        for j in range(n):
            mix_send[t, j] = outbox[j * capacity : (j + 1) * capacity].astype(BF16)
        mix_recv[t, ep] = mix_send[t, ep]
        ep_scatter(s_mix, mix_send.at[t], mix_recv.at[t], r_mix + t)
        middle.append(part.astype(F32))
    middle = jnp.concatenate(middle, axis=1)
    for t in range(m):
        mid_cols[t] = middle[:, t * out_cols : (t + 1) * out_cols]

    phase_name("side")
    normed_mix = rms_scale(middle, mix_gain).astype(BF16)
    side_load.wait()
    side_down_load.wait()
    side_hidden = silu(
        jnp.dot(normed_mix, side_w[0], preferred_element_type=F32)
    ) * jnp.dot(normed_mix, side_w[1], preferred_element_type=F32)
    side_term = jnp.dot(side_hidden.astype(BF16), side_down_w[...], preferred_element_type=F32)
    switch = jnp.sum(normed_mix.astype(F32) * branch_gate, axis=1, keepdims=True)
    switch = 1.0 / (1.0 + jnp.exp(-switch))
    for t in range(m):
        side_cols[t] = switch * side_term[:, t * out_cols : (t + 1) * out_cols]
    for d in range(1, m):
        t = lax.rem(tp + d, m)
        side_send[d - 1] = side_cols[t].astype(BF16)
        remote(s_side, side_send.at[d - 1], side_recv.at[d - 1], (ep, t))

    phase_name("new_keys")
    arrived(s_proj, proj_recv.at[:, others])
    key_rows = collect(proj_recv.at[0])
    for h in range(heads):
        part = slice(h * dh, (h + 1) * dh)
        new_keys_ref[:, part] = rms_scale(key_rows[:, part], 1.0).astype(BF16)
    new_values_ref[...] = collect(proj_recv.at[1]).astype(BF16)
    expert_load.wait()
    down_load.wait()
    sent(s_col, col_send.at[others])
    sent(s_query, query_send.at[:, others])
    sent(s_proj, proj_send.at[:, others])
    sent(s_reduce, reduce_buf.at[:, fellows])

    gate_pre = up_pre = squares = None
    for t in range(parts):
        phase_name("rows_wait")
        arrived(r_mix + t, mix_recv.at[t, others])
        phase_name("expert")
        for j in range(n):
            slot_rows[t, j * capacity : (j + 1) * capacity, :] = mix_recv[t, j].astype(F32)
        span = slice(t * part_cols, (t + 1) * part_cols)
        rows = slot_rows[t]
        square = jnp.sum(rows * rows, axis=1, keepdims=True)
        rows = (rows * mix_gain[:, span]).astype(BF16)
        gate_part = jnp.dot(rows, expert_w[0, span, :], preferred_element_type=F32)
        up_part = jnp.dot(rows, expert_w[1, span, :], preferred_element_type=F32)
        gate_pre = gate_part if t == 0 else gate_pre + gate_part
        up_pre = up_part if t == 0 else up_pre + up_part
        squares = square if t == 0 else squares + square
    factor = lax.rsqrt(squares / width + epsilon)
    hidden = (silu(gate_pre * factor) * (up_pre * factor)).astype(BF16)
    for t in range(m):
        expert_term = jnp.dot(
            hidden, down_w[:, t * out_cols : (t + 1) * out_cols], preferred_element_type=F32
        )
        for j in range(n):
            back_send[t, j] = expert_term[j * capacity : (j + 1) * capacity].astype(BF16)
        for k in range(n - 1):
            j = k + (k - ep + n) // n
            remote(s_back, back_send.at[t, j], back_recv.at[tp, ep], (j, t))
    for d in range(1, m):
        t = lax.rem(tp + d, m)
        remote(s_near, back_send.at[t, ep], back_recv.at[tp, ep], (ep, t))
    back_recv[tp, ep] = back_send[tp, ep]
    phase_name("side_wait")
    result = mid_cols[tp] + side_cols[tp]
    arrived(s_side, side_recv.at[...])
    for d in range(1, m):
        result = result + side_recv[d - 1].astype(F32)
    sent(s_mix, mix_send.at[:, others])
    sent(s_side, side_send.at[...])
    phase_name("back_wait")
    arrived(s_near, back_recv.at[fellows, 0])
    arrived(s_back, back_recv.at[:, others])
    phase_name("combine")
    for j in range(n):
        slot_cols[j * capacity : (j + 1) * capacity, :] = sum(
            back_recv[i, j].astype(F32) for i in range(m)
        )
    chosen = jnp.dot(route_map, slot_cols[...].astype(BF16), preferred_element_type=F32)
    for k, w in enumerate(weights):
        result = result + w * chosen[k * seqs : (k + 1) * seqs]
    mixed_ref[...] = result.astype(BF16)
    phase_name("drain")
    sent(s_near, back_send.at[fellows, 0])
    sent(s_back, back_send.at[:, others])
    phase_name(None)


def hand_on(count, *refs):
    sources, targets, sem = refs[:count], refs[count : 2 * count], refs[-1]
    copies = [
        pltpu.make_async_copy(src, dst, sem.at[i])
        for i, (src, dst) in enumerate(zip(sources, targets))
    ]
    for copy in copies:
        copy.start()
    for copy in copies:
        copy.wait()


def fused(n, m, *args):
    (
        tokens,
        attn_gain,
        query_weight,
        key_weight,
        value_weight,
        query_gain,
        stick_bias,
        key_cache,
        value_cache,
        lengths,
        out_weight,
        mix_gain,
        route_ids,
        route_weights,
        expert_gate,
        expert_up,
        expert_down,
        side_gate,
        side_up,
        side_down,
        branch_gate,
    ) = args
    seqs, width = tokens.shape
    _, heads, slots, dh = key_cache.shape
    head_cols = query_weight.shape[1]
    out_cols = width // m
    capacity = max(2, 2 * route_ids.shape[1] * seqs // n)
    parts = 2
    vmem = pl.BlockSpec(memory_space=pltpu.VMEM)
    hbm = pl.BlockSpec(memory_space=pl.ANY)
    dma = pltpu.SemaphoreType.DMA

    def scratch(*shape, dtype=BF16):
        return pltpu.VMEM(shape, dtype)

    small = (
        tokens,
        attn_gain.reshape(1, width),
        query_gain.reshape(1, dh),
        stick_bias.reshape(1, heads),
        lengths.reshape(1, seqs),
        mix_gain.reshape(1, width),
        route_ids.T,
        route_weights.T,
        branch_gate.reshape(1, width),
    )
    shapes = ((seqs, out_cols), (seqs, head_cols), (seqs, head_cols))
    outs = pl.pallas_call(
        lambda *refs: layer_kernel(n, m, *refs),
        out_shape=tuple(pltpu.VMEM(shape, BF16) for shape in shapes),
        in_specs=[hbm] * 21,
        out_specs=(vmem, vmem, vmem),
        scratch_shapes=[
            scratch(seqs, width),
            scratch(3, 1, width, dtype=F32),
            *(scratch(*x.shape, dtype=x.dtype) for x in (*small[2:5], *small[6:8])),
            scratch(3, *query_weight.shape),
            scratch(*key_cache.shape),
            scratch(heads, seqs, dh, slots),
            scratch(heads, seqs, slots, dh),
            scratch(*out_weight.shape),
            scratch(2, *expert_gate.shape[1:]),
            scratch(*expert_down.shape[1:]),
            scratch(2, *side_gate.shape),
            scratch(*side_down.shape),
            scratch(n, seqs, width // n),
            scratch(n, seqs, width // n),
            scratch(2, n, seqs, head_cols // 2),
            scratch(2, n, seqs, head_cols // 2),
            scratch(2, n, seqs, head_cols),
            scratch(2, n, seqs, head_cols),
            scratch(parts, m, seqs, width // parts),
            scratch(m, seqs, out_cols, dtype=F32),
            scratch(parts, n, capacity, width // parts),
            scratch(parts, n, capacity, width // parts),
            scratch(parts, n * capacity, width // parts, dtype=F32),
            scratch(n * capacity, out_cols, dtype=F32),
            scratch(m, seqs, out_cols, dtype=F32),
            scratch(m - 1, seqs, out_cols),
            scratch(m - 1, seqs, out_cols),
            scratch(m, n, capacity, out_cols),
            scratch(m, n, capacity, out_cols),
            dma((15,)),
            dma((8,)),
            dma((10 + 2 * parts,)),
        ],
        compiler_params=pltpu.CompilerParams(
            collective_id=0, has_side_effects=True, vmem_limit_bytes=60 * 1024 * 1024
        ),
        name="layer",
    )(
        *small,
        query_weight,
        key_weight,
        value_weight,
        key_cache,
        value_cache,
        out_weight,
        expert_gate,
        expert_up,
        expert_down,
        side_gate,
        side_up,
        side_down,
    )
    return pl.pallas_call(
        lambda *refs: hand_on(len(shapes), *refs),
        out_shape=tuple(jax.ShapeDtypeStruct(shape, BF16) for shape in shapes),
        in_specs=[vmem] * len(shapes),
        out_specs=(hbm,) * len(shapes),
        scratch_shapes=[dma((len(shapes),))],
        name="hand_on",
    )(*(pltpu.with_memory_space_constraint(x, pltpu.VMEM) for x in outs))


def layer(n, m, *args):
    tokens, query_weight, key_cache = args[0], args[2], args[7]
    expert_gate, side_gate = args[14], args[17]
    seqs, width = tokens.shape
    lanes = (width // n, width // m, query_weight.shape[1], key_cache.shape[2])
    lanes += (key_cache.shape[3], expert_gate.shape[2], side_gate.shape[1])
    lanes += (query_weight.shape[1] // 2,)
    rows = (seqs, key_cache.shape[1])
    held = 2 * sum(a.size for a in args[2:] if a.dtype == BF16) + 2 * key_cache.size
    aligned = all(x % 128 == 0 for x in lanes) and all(x % 8 == 0 for x in rows)
    if n > 1 and m > 1 and aligned and expert_gate.shape[0] == 1 and held < 48 * 1024 * 1024:
        return fused(n, m, *args)
    return body(*args)


def solution(mesh):
    in_specs = (
        P("ep", None),
        P(),
        P("ep", "tp"),
        P("ep", "tp"),
        P("ep", "tp"),
        P(),
        P("tp"),
        P("ep", "tp", None, None),
        P("ep", "tp", None, None),
        P("ep"),
        P("tp", None),
        P(),
        P("ep", None),
        P("ep", None),
        P("ep", None, "tp"),
        P("ep", None, "tp"),
        P("ep", "tp", None),
        P(None, "tp"),
        P(None, "tp"),
        P("tp", None),
        P(),
    )
    out_specs = (P("ep", "tp"), P("ep", "tp"), P("ep", "tp"))
    return jax.shard_map(
        lambda *args: layer(mesh.shape["ep"], mesh.shape["tp"], *args),
        mesh=mesh,
        in_specs=in_specs,
        out_specs=out_specs,
        check_vma=False,
    )
```

time: 42.2 us -> 31.9 us (0.76)
  Pallas kernels: 41.3 us -> 31.1 us
    pallas_call x2, Pallas kernels: 41.3 us -> 31.1 us  [the longest x1 30.4 us: fused(): pl.pallas_call(lambda *refs: layer_kernel(n, m, *refs), out_shape=tuple((...]
where the time goes in v1:
time: 31.9 us; the launch traced here: 31.7 us
  Pallas kernels  31.1 us (97%)
  between operations  0.65 us (2%)
    pallas_call x1, Pallas kernels, fused(): pl.pallas_call(lambda *refs: layer_kernel(n, m, *refs), out_shape=tuple((...  30.4 us
    pallas_call x1, Pallas kernels, fused(): pl.pallas_call(lambda *refs: hand_on(len(shapes), *refs), out_shape=tuple...  0.64 us

profile of v1, /device:TPU:0, one launch (start us, length us, event | category | flops | bytes accessed | tf_op | source)
XLA Modules:
  0.0 31.7 jit_solution(9899183641504318911)
XLA Ops:
  0.6 30.4 %layer.1 = (bf16[8,512]{1,0:T(8,128)(2,1)S(1)}, bf16[8,1024]{1,0:T(8,128)(2,1)S(1)}, bf16[8,1024]{1,0:T(8,128)(2,1)S(1)}) custom-call(bf16[8,2048]{1,0:T(8,128)(2,1)} %refs_0_.1, f32[1,2048]{1,0:T(1,128)} %bitcast.8, f32[1,128]{1,0:T(1,128)} %bitcast.13, f32[1,8]{1,0:T(1,128)} %bitcast.14, s32[1,8]{1,0:T(1,128)} %bitcast.15, f32[1,2048]{1,0:T(1,128)} %bitcast.9, ...), custom_call_target="tpu_custom_call" | custom-call | tf_op jit(solution)/shard_map/layer/pallas_call | solution.py:622
  31.1 0.6 %hand_on.1 = (bf16[8,512]{1,0:T(8,128)(2,1)}, bf16[8,1024]{1,0:T(8,128)(2,1)}, bf16[8,1024]{1,0:T(8,128)(2,1)}) custom-call(bf16[8,512]{1,0:T(8,128)(2,1)S(1)} %get-tuple-element.6.refs_0_, bf16[8,1024]{1,0:T(8,128)(2,1)S(1)} %get-tuple-element.7.refs_1_, bf16[8,1024]{1,0:T(8,128)(2,1)S(1)} %get-tuple-element.8.refs_2_), custom_call_target="tpu_custom_call" | custom-call | tf_op jit(solution)/shard_map/hand_on/pallas_call | solution.py:680

commit v2 on v1

--- a/solution.py
+++ b/solution.py
@@ -231,6 +231,7 @@
     mix_send,
     mix_recv,
     slot_rows,
+    pre,
     slot_cols,
     side_cols,
     side_send,
@@ -252,20 +253,19 @@
 
     phase_name = Phases()
     phase_name("greet")
+    def load(k, whole, *pairs, priority=1):
+        for src, dst in pairs:
+            pltpu.make_async_copy(src, dst, load_sem.at[k]).start(priority=priority)
+        return pltpu.make_async_copy(whole, whole, load_sem.at[k])
+
+    tokens_load = load(0, tokens_ref, (tokens_hbm, tokens_ref), priority=0)
+    gains = (attn_gain_hbm, mix_gain_hbm, branch_hbm)
+    rows_load = load(1, rows_ref, *((x, rows_ref.at[i]) for i, x in enumerate(gains)), priority=0)
     barrier = pltpu.get_barrier_semaphore()
     for d in range(1, n):
         pl.semaphore_signal(barrier, inc=1, device_id=(lax.rem(ep + d, n), tp), device_id_type=MESH)
     for d in range(1, m):
         pl.semaphore_signal(barrier, inc=1, device_id=(ep, lax.rem(tp + d, m)), device_id_type=MESH)
-
-    def load(k, whole, *pairs, priority=1):
-        for src, dst in pairs:
-            pltpu.make_async_copy(src, dst, load_sem.at[k]).start(priority=priority)
-        return pltpu.make_async_copy(whole, whole, load_sem.at[k])
-
-    tokens_load = load(0, tokens_ref, (tokens_hbm, tokens_ref), priority=0)
-    gains = (attn_gain_hbm, mix_gain_hbm, branch_hbm)
-    rows_load = load(1, rows_ref, *((x, rows_ref.at[i]) for i, x in enumerate(gains)), priority=0)
     small = (
         (ids_hbm, ids_ref),
         (weights_hbm, weights_ref),
@@ -300,15 +300,24 @@
     def arrived(sem, whole):
         pltpu.make_async_copy(whole, whole, recv_sem.at[sem]).wait()
 
+    upper = ep // (n // 2)
+    far_first = []
+    for k in range(n - 1):
+        low = n - 2 - k + (n - 1 - k - ep + n - 1) // n
+        high = k + (k - ep + n) // n
+        far_first.append((1 - upper) * low + upper * high)
+
     def ep_scatter(sem, send, recv, arrival=None):
-        for d in range(1, n):
-            j = lax.rem(ep + d, n)
+        for j in far_first:
             remote(sem, send.at[j], recv.at[ep], (j, tp), arrival)
 
     others = pl.ds(0, n - 1)
     fellows = pl.ds(0, m - 1)
-    s_col, s_query, s_proj, s_reduce, s_mix, s_side, s_back, s_near = range(8)
-    r_query, r_reduce, r_mix = 8, 10, 10 + parts
+    groups = query_send.shape[0]
+    s_first, s_plane, s_rows, s_proj = range(4)
+    r_col, r_proj, r_side, r_back, r_near, r_query = range(6)
+    r_reduce = r_query + groups
+    r_mix = r_reduce + parts
 
     tokens_load.wait()
     rows_load.wait()
@@ -321,7 +330,7 @@
     phase_name("barrier")
     pl.semaphore_wait(barrier, (n - 1) + (m - 1))
     phase_name("col_send")
-    ep_scatter(s_col, col_send, col_recv)
+    ep_scatter(s_first, col_send, col_recv, r_col)
 
     for copy in small_loads:
         copy.wait()
@@ -357,25 +366,24 @@
     ).astype(BF16)
     proj_load.wait()
     phase_name("col_wait")
-    arrived(s_col, col_recv.at[others])
+    arrived(r_col, col_recv.at[others])
     phase_name("project")
     picked = stack_rows(col_recv).astype(BF16)
 
     half = query_send.shape[3]
-    for g in range(2):
-        part = jnp.dot(
-            picked, proj_w[0, :, g * half : (g + 1) * half], preferred_element_type=F32
-        )
+    part = jnp.dot(picked, proj_w[0], preferred_element_type=F32).astype(BF16)
+    sent(s_first, col_send.at[others])
+    for g in range(groups):
         for j in range(n):
-            query_send[g, j] = part[j * seqs : (j + 1) * seqs].astype(BF16)
+            query_send[g, j] = part[j * seqs : (j + 1) * seqs, g * half : (g + 1) * half]
         query_recv[g, ep] = query_send[g, ep]
-        ep_scatter(s_query, query_send.at[g], query_recv.at[g], r_query + g)
+        ep_scatter(s_first, query_send.at[g], query_recv.at[g], r_query + g)
     phase_name("turn")
-    out_load = load(10, out_w, (out_hbm, out_w))
-    side_load = load(11, side_w, (side_gate_hbm, side_w.at[0]), (side_up_hbm, side_w.at[1]))
-    side_down_load = load(12, side_down_w, (side_down_hbm, side_down_w))
-    expert_load = load(13, expert_w, (gate_hbm.at[0], expert_w.at[0]), (up_hbm.at[0], expert_w.at[1]))
-    down_load = load(14, down_w, (down_hbm.at[0], down_w))
+    out_load = load(0, out_w, (out_hbm, out_w))
+    side_load = load(1, side_w, (side_gate_hbm, side_w.at[0]), (side_up_hbm, side_w.at[1]))
+    side_down_load = load(2, side_down_w, (side_down_hbm, side_down_w))
+    expert_load = load(3, expert_w, (gate_hbm.at[0], expert_w.at[0]), (up_hbm.at[0], expert_w.at[1]))
+    down_load = load(4, down_w, (down_hbm.at[0], down_w))
     for i in (1, 2):
         part = jnp.dot(picked, proj_w[i], preferred_element_type=F32)
         for j in range(n):
@@ -401,14 +409,14 @@
     scale = dh ** (-0.5)
     some = half // dh
     score_rows, rest_rows = [], []
-    for g in range(2):
+    for g in range(groups):
         phase_name("query_wait")
         arrived(r_query + g, query_recv.at[g, others])
         phase_name("scores")
         query = collect(query_recv.at[g])
         if g == 0:
             for i in range(2):
-                ep_scatter(s_proj, proj_send.at[i], proj_recv.at[i])
+                ep_scatter(s_proj, proj_send.at[i], proj_recv.at[i], r_proj)
         for k in range(some):
             h = g * some + k
             q = rms_scale(query[:, k * dh : (k + 1) * dh], query_gain_ref[...])
@@ -452,7 +460,7 @@
         ).astype(BF16)
         for d in range(1, m):
             own = reduce_buf.at[t, tp]
-            remote(s_reduce, own, own, (ep, lax.rem(tp + d, m)), r_reduce + t)
+            remote(s_plane, own, own, (ep, lax.rem(tp + d, m)), r_reduce + t)
 
     middle = []
     for t in range(parts):
@@ -465,7 +473,7 @@
         for j in range(n):
             mix_send[t, j] = outbox[j * capacity : (j + 1) * capacity].astype(BF16)
         mix_recv[t, ep] = mix_send[t, ep]
-        ep_scatter(s_mix, mix_send.at[t], mix_recv.at[t], r_mix + t)
+        ep_scatter(s_rows, mix_send.at[t], mix_recv.at[t], r_mix + t)
         middle.append(part.astype(F32))
     middle = jnp.concatenate(middle, axis=1)
     for t in range(m):
@@ -483,26 +491,18 @@
     switch = 1.0 / (1.0 + jnp.exp(-switch))
     for t in range(m):
         side_cols[t] = switch * side_term[:, t * out_cols : (t + 1) * out_cols]
+    sent(s_plane, reduce_buf.at[:, fellows])
     for d in range(1, m):
         t = lax.rem(tp + d, m)
         side_send[d - 1] = side_cols[t].astype(BF16)
-        remote(s_side, side_send.at[d - 1], side_recv.at[d - 1], (ep, t))
-
-    phase_name("new_keys")
-    arrived(s_proj, proj_recv.at[:, others])
-    key_rows = collect(proj_recv.at[0])
-    for h in range(heads):
-        part = slice(h * dh, (h + 1) * dh)
-        new_keys_ref[:, part] = rms_scale(key_rows[:, part], 1.0).astype(BF16)
-    new_values_ref[...] = collect(proj_recv.at[1]).astype(BF16)
+        remote(s_plane, side_send.at[d - 1], side_recv.at[d - 1], (ep, t), r_side)
+
+    phase_name("settle")
     expert_load.wait()
     down_load.wait()
-    sent(s_col, col_send.at[others])
-    sent(s_query, query_send.at[:, others])
-    sent(s_proj, proj_send.at[:, others])
-    sent(s_reduce, reduce_buf.at[:, fellows])
-
-    gate_pre = up_pre = squares = None
+    sent(s_first, query_send.at[:, others])
+
+    squares = None
     for t in range(parts):
         phase_name("rows_wait")
         arrived(r_mix + t, mix_recv.at[t, others])
@@ -513,11 +513,14 @@
         rows = slot_rows[t]
         square = jnp.sum(rows * rows, axis=1, keepdims=True)
         rows = (rows * mix_gain[:, span]).astype(BF16)
-        gate_part = jnp.dot(rows, expert_w[0, span, :], preferred_element_type=F32)
-        up_part = jnp.dot(rows, expert_w[1, span, :], preferred_element_type=F32)
-        gate_pre = gate_part if t == 0 else gate_pre + gate_part
-        up_pre = up_part if t == 0 else up_pre + up_part
+        for i in range(2):
+            share = jnp.dot(rows, expert_w[i, span, :], preferred_element_type=F32)
+            pre[i] = share if t == 0 else pre[i] + share
         squares = square if t == 0 else squares + square
+        if t == 0:
+            sent(s_plane, side_send.at[...])
+    sent(s_rows, mix_send.at[:, others])
+    gate_pre, up_pre = pre[0], pre[1]
     factor = lax.rsqrt(squares / width + epsilon)
     hidden = (silu(gate_pre * factor) * (up_pre * factor)).astype(BF16)
     for t in range(m):
@@ -528,21 +531,27 @@
             back_send[t, j] = expert_term[j * capacity : (j + 1) * capacity].astype(BF16)
         for k in range(n - 1):
             j = k + (k - ep + n) // n
-            remote(s_back, back_send.at[t, j], back_recv.at[tp, ep], (j, t))
+            remote(s_rows, back_send.at[t, j], back_recv.at[tp, ep], (j, t), r_back)
     for d in range(1, m):
         t = lax.rem(tp + d, m)
-        remote(s_near, back_send.at[t, ep], back_recv.at[tp, ep], (ep, t))
+        remote(s_plane, back_send.at[t, ep], back_recv.at[tp, ep], (ep, t), r_near)
     back_recv[tp, ep] = back_send[tp, ep]
     phase_name("side_wait")
     result = mid_cols[tp] + side_cols[tp]
-    arrived(s_side, side_recv.at[...])
+    arrived(r_side, side_recv.at[...])
     for d in range(1, m):
         result = result + side_recv[d - 1].astype(F32)
-    sent(s_mix, mix_send.at[:, others])
-    sent(s_side, side_send.at[...])
+    phase_name("new_keys")
+    arrived(r_proj, proj_recv.at[:, others])
+    key_rows = collect(proj_recv.at[0])
+    for h in range(heads):
+        part = slice(h * dh, (h + 1) * dh)
+        new_keys_ref[:, part] = rms_scale(key_rows[:, part], 1.0).astype(BF16)
+    new_values_ref[...] = collect(proj_recv.at[1]).astype(BF16)
+    sent(s_proj, proj_send.at[:, others])
     phase_name("back_wait")
-    arrived(s_near, back_recv.at[fellows, 0])
-    arrived(s_back, back_recv.at[:, others])
+    arrived(r_near, back_recv.at[fellows, 0])
+    arrived(r_back, back_recv.at[:, others])
     phase_name("combine")
     for j in range(n):
         slot_cols[j * capacity : (j + 1) * capacity, :] = sum(
@@ -553,8 +562,8 @@
         result = result + w * chosen[k * seqs : (k + 1) * seqs]
     mixed_ref[...] = result.astype(BF16)
     phase_name("drain")
-    sent(s_near, back_send.at[fellows, 0])
-    sent(s_back, back_send.at[:, others])
+    sent(s_plane, back_send.at[fellows, 0])
+    sent(s_rows, back_send.at[:, others])
     phase_name(None)
 
 
@@ -600,6 +609,7 @@
     out_cols = width // m
     capacity = max(2, 2 * route_ids.shape[1] * seqs // n)
     parts = 2
+    groups = 2
     vmem = pl.BlockSpec(memory_space=pltpu.VMEM)
     hbm = pl.BlockSpec(memory_space=pl.ANY)
     dma = pltpu.SemaphoreType.DMA
@@ -639,8 +649,8 @@
             scratch(*side_down.shape),
             scratch(n, seqs, width // n),
             scratch(n, seqs, width // n),
-            scratch(2, n, seqs, head_cols // 2),
-            scratch(2, n, seqs, head_cols // 2),
+            scratch(groups, n, seqs, head_cols // groups),
+            scratch(groups, n, seqs, head_cols // groups),
             scratch(2, n, seqs, head_cols),
             scratch(2, n, seqs, head_cols),
             scratch(parts, m, seqs, width // parts),
@@ -648,15 +658,16 @@
             scratch(parts, n, capacity, width // parts),
             scratch(parts, n, capacity, width // parts),
             scratch(parts, n * capacity, width // parts, dtype=F32),
+            scratch(2, n * capacity, expert_gate.shape[2], dtype=F32),
             scratch(n * capacity, out_cols, dtype=F32),
             scratch(m, seqs, out_cols, dtype=F32),
             scratch(m - 1, seqs, out_cols),
             scratch(m - 1, seqs, out_cols),
             scratch(m, n, capacity, out_cols),
             scratch(m, n, capacity, out_cols),
-            dma((15,)),
-            dma((8,)),
-            dma((10 + 2 * parts,)),
+            dma((10,)),
+            dma((4,)),
+            dma((5 + groups + 2 * parts,)),
         ],
         compiler_params=pltpu.CompilerParams(
             collective_id=0, has_side_effects=True, vmem_limit_bytes=60 * 1024 * 1024
@@ -693,7 +704,7 @@
     seqs, width = tokens.shape
     lanes = (width // n, width // m, query_weight.shape[1], key_cache.shape[2])
     lanes += (key_cache.shape[3], expert_gate.shape[2], side_gate.shape[1])
-    lanes += (query_weight.shape[1] // 2,)
+    lanes += (query_weight.shape[1] // 2, width // 2)
     rows = (seqs, key_cache.shape[1])
     held = 2 * sum(a.size for a in args[2:] if a.dtype == BF16) + 2 * key_cache.size
     aligned = all(x % 128 == 0 for x in lanes) and all(x % 8 == 0 for x in rows)

time: 31.9 us -> 31.4 us (0.984)
  Pallas kernels: 31.1 us -> 30.6 us
    pallas_call x1, Pallas kernels: 30.4 us -> 29.9 us  [fused(): pl.pallas_call(lambda *refs: layer_kernel(n, m, *refs), out_shape=tuple((...]
where the time goes in v2:
time: 31.4 us; the launch traced here: 31.2 us
  Pallas kernels  30.6 us (97%)
  between operations  0.65 us (2%)
    pallas_call x1, Pallas kernels, fused(): pl.pallas_call(lambda *refs: layer_kernel(n, m, *refs), out_shape=tuple((...  29.9 us
    pallas_call x1, Pallas kernels, fused(): pl.pallas_call(lambda *refs: hand_on(len(shapes), *refs), out_shape=tuple...  0.64 us

profile of v2, /device:TPU:0, one launch (start us, length us, event | category | flops | bytes accessed | tf_op | source)
XLA Modules:
  0.0 31.2 jit_solution(838353892766241376)
XLA Ops:
  0.6 29.9 %layer.1 = (bf16[8,512]{1,0:T(8,128)(2,1)S(1)}, bf16[8,1024]{1,0:T(8,128)(2,1)S(1)}, bf16[8,1024]{1,0:T(8,128)(2,1)S(1)}) custom-call(bf16[8,2048]{1,0:T(8,128)(2,1)} %refs_0_.1, f32[1,2048]{1,0:T(1,128)} %bitcast.8, f32[1,128]{1,0:T(1,128)} %bitcast.13, f32[1,8]{1,0:T(1,128)} %bitcast.14, s32[1,8]{1,0:T(1,128)} %bitcast.15, f32[1,2048]{1,0:T(1,128)} %bitcast.9, ...), custom_call_target="tpu_custom_call" | custom-call | tf_op jit(solution)/shard_map/layer/pallas_call | solution.py:632
  30.6 0.6 %hand_on.1 = (bf16[8,512]{1,0:T(8,128)(2,1)}, bf16[8,1024]{1,0:T(8,128)(2,1)}, bf16[8,1024]{1,0:T(8,128)(2,1)}) custom-call(bf16[8,512]{1,0:T(8,128)(2,1)S(1)} %get-tuple-element.6.refs_0_, bf16[8,1024]{1,0:T(8,128)(2,1)S(1)} %get-tuple-element.7.refs_1_, bf16[8,1024]{1,0:T(8,128)(2,1)S(1)} %get-tuple-element.8.refs_2_), custom_call_target="tpu_custom_call" | custom-call | tf_op jit(solution)/shard_map/hand_on/pallas_call | solution.py:691

commit v3 on v2

--- a/solution.py
+++ b/solution.py
@@ -175,6 +175,17 @@
 
 def stack_rows(buffer):
     return jnp.concatenate([buffer[i].astype(F32) for i in range(buffer.shape[0])], axis=0)
+
+
+def vector_products(rows, blocks):
+    columns = rows.astype(BF16).astype(F32).T
+    return jnp.concatenate(
+        [
+            jnp.sum(blocks[s].astype(F32) * columns[:, s : s + 1], axis=0, keepdims=True)
+            for s in range(rows.shape[0])
+        ],
+        axis=0,
+    )
 
 
 def layer_kernel(
@@ -420,12 +431,15 @@
         for k in range(some):
             h = g * some + k
             q = rms_scale(query[:, k * dh : (k + 1) * dh], query_gain_ref[...])
-            spread = jnp.concatenate(
-                [jnp.where(query_row == s, q, 0.0).astype(BF16) for s in range(seqs)], axis=1
-            )
-            score = jnp.dot(
-                spread, turned[h].reshape(seqs * dh, slots), preferred_element_type=F32
-            )
+            if k == some - 1:
+                score = vector_products(q, turned.at[h])
+            else:
+                spread = jnp.concatenate(
+                    [jnp.where(query_row == s, q, 0.0).astype(BF16) for s in range(seqs)], axis=1
+                )
+                score = jnp.dot(
+                    spread, turned[h].reshape(seqs * dh, slots), preferred_element_type=F32
+                )
             score = score * scale + bias_ref[0:1, h : h + 1]
             full = -softplus(score)
             score_rows.append(score + full)
@@ -445,6 +459,9 @@
         stick = jnp.where(
             visible, jnp.exp(score_rows[h] + between[h * seqs : (h + 1) * seqs]), 0.0
         )
+        if h == 0:
+            attended.append(vector_products(stick, values.at[h]))
+            continue
         spread = jnp.concatenate(
             [jnp.where(slot_row == s, stick, 0.0).astype(BF16) for s in range(seqs)], axis=1
         )

time: 31.4 us -> 31 us (0.987)
  Pallas kernels: 30.6 us -> 30.2 us
where the time goes in v3:
time: 31 us; the launch traced here: 30.9 us
  Pallas kernels  30.2 us (97%)
  between operations  0.65 us (2%)
    pallas_call x1, Pallas kernels, fused(): pl.pallas_call(lambda *refs: layer_kernel(n, m, *refs), out_shape=tuple((...  29.6 us
    pallas_call x1, Pallas kernels, fused(): pl.pallas_call(lambda *refs: hand_on(len(shapes), *refs), out_shape=tuple...  0.64 us

profile of v3, /device:TPU:0, one launch (start us, length us, event | category | flops | bytes accessed | tf_op | source)
XLA Modules:
  0.0 30.9 jit_solution(2582677449357475757)
XLA Ops:
  0.6 29.6 %layer.1 = (bf16[8,512]{1,0:T(8,128)(2,1)S(1)}, bf16[8,1024]{1,0:T(8,128)(2,1)S(1)}, bf16[8,1024]{1,0:T(8,128)(2,1)S(1)}) custom-call(bf16[8,2048]{1,0:T(8,128)(2,1)} %refs_0_.1, f32[1,2048]{1,0:T(1,128)} %bitcast.8, f32[1,128]{1,0:T(1,128)} %bitcast.13, f32[1,8]{1,0:T(1,128)} %bitcast.14, s32[1,8]{1,0:T(1,128)} %bitcast.15, f32[1,2048]{1,0:T(1,128)} %bitcast.9, ...), custom_call_target="tpu_custom_call" | custom-call | tf_op jit(solution)/shard_map/layer/pallas_call | solution.py:649
  30.3 0.6 %hand_on.1 = (bf16[8,512]{1,0:T(8,128)(2,1)}, bf16[8,1024]{1,0:T(8,128)(2,1)}, bf16[8,1024]{1,0:T(8,128)(2,1)}) custom-call(bf16[8,512]{1,0:T(8,128)(2,1)S(1)} %get-tuple-element.6.refs_0_, bf16[8,1024]{1,0:T(8,128)(2,1)S(1)} %get-tuple-element.7.refs_1_, bf16[8,1024]{1,0:T(8,128)(2,1)S(1)} %get-tuple-element.8.refs_2_), custom_call_target="tpu_custom_call" | custom-call | tf_op jit(solution)/shard_map/hand_on/pallas_call | solution.py:708

commit v4 on v3

--- a/solution.py
+++ b/solution.py
@@ -446,14 +446,12 @@
             rest_rows.append(jnp.where(visible, full, 0.0))
     rest = jnp.concatenate(rest_rows, axis=0)
     high = rest.astype(BF16)
-    left = rest - high.astype(F32)
-    middle_part = left.astype(BF16)
-    low = (left - middle_part.astype(F32)).astype(BF16)
+    low = (rest - high.astype(F32)).astype(BF16)
     pieces = jnp.dot(
-        jnp.concatenate([high, middle_part, low], axis=0), later, preferred_element_type=F32
+        jnp.concatenate([high, low], axis=0), later, preferred_element_type=F32
     )
     count = seqs * heads
-    between = pieces[:count] + pieces[count : 2 * count] + pieces[2 * count :]
+    between = pieces[:count] + pieces[count:]
     attended = []
     for h in range(heads):
         stick = jnp.where(

time: 31 us -> 31 us (level)
  no operation moved by 1% of the time
where the time goes in v4:
time: 31 us; the launch traced here: 30.8 us
  Pallas kernels  30.2 us (97%)
  between operations  0.65 us (2%)
    pallas_call x1, Pallas kernels, fused(): pl.pallas_call(lambda *refs: layer_kernel(n, m, *refs), out_shape=tuple((...  29.5 us
    pallas_call x1, Pallas kernels, fused(): pl.pallas_call(lambda *refs: hand_on(len(shapes), *refs), out_shape=tuple...  0.64 us

profile of v4, /device:TPU:0, one launch (start us, length us, event | category | flops | bytes accessed | tf_op | source)
XLA Modules:
  0.0 30.8 jit_solution(2283478906272821847)
XLA Ops:
  0.6 29.5 %layer.1 = (bf16[8,512]{1,0:T(8,128)(2,1)S(1)}, bf16[8,1024]{1,0:T(8,128)(2,1)S(1)}, bf16[8,1024]{1,0:T(8,128)(2,1)S(1)}) custom-call(bf16[8,2048]{1,0:T(8,128)(2,1)} %refs_0_.1, f32[1,2048]{1,0:T(1,128)} %bitcast.8, f32[1,128]{1,0:T(1,128)} %bitcast.13, f32[1,8]{1,0:T(1,128)} %bitcast.14, s32[1,8]{1,0:T(1,128)} %bitcast.15, f32[1,2048]{1,0:T(1,128)} %bitcast.9, ...), custom_call_target="tpu_custom_call" | custom-call | tf_op jit(solution)/shard_map/layer/pallas_call | solution.py:647
  30.2 0.6 %hand_on.1 = (bf16[8,512]{1,0:T(8,128)(2,1)}, bf16[8,1024]{1,0:T(8,128)(2,1)}, bf16[8,1024]{1,0:T(8,128)(2,1)}) custom-call(bf16[8,512]{1,0:T(8,128)(2,1)S(1)} %get-tuple-element.6.refs_0_, bf16[8,1024]{1,0:T(8,128)(2,1)S(1)} %get-tuple-element.7.refs_1_, bf16[8,1024]{1,0:T(8,128)(2,1)S(1)} %get-tuple-element.8.refs_2_), custom_call_target="tpu_custom_call" | custom-call | tf_op jit(solution)/shard_map/hand_on/pallas_call | solution.py:706
